TPU v7x, 32 devices: a whole 2x2x4 slice. The times are simulated.
32 devices in a mesh: sp: 16 (over z, y, x), tp: 2 (over core).
Axes of the slice: x: 2, y: 2, z: 4, core: 2. Of those that a mesh axis runs over, the one named last changes fastest.
Arguments:
- latent: bfloat16 [4096, 256], P('sp'), may hold values from -6 to 6
- rotary_key: bfloat16 [4096, 64], P('sp'), may hold values from -7 to 7
- doc_ids: int32 [4096], P('sp'), may hold values from 0 to 7, never falling along the last dimension, each value on 1 to 1024 neighbouring positions
- queries_content: bfloat16 [4096, 1024], P('sp', 'tp'), may hold values from -6 to 6
- queries_rotary: bfloat16 [4096, 512], P('sp', 'tp'), may hold values from -400 to 400
- w_key_up: bfloat16 [256, 1024], replicated, may hold values from -0.375 to 0.375
- w_value_up: bfloat16 [256, 1024], replicated, may hold values from -0.375 to 0.375
- w_out: bfloat16 [1024, 2048], P('tp'), may hold values from -1.5 to 1.5
- residual: bfloat16 [4096, 2048], P(('sp', 'tp')), may hold values from -4 to 4
- norm_gain: float32 [2048], replicated, may hold values from 0.1 to 1.9
- routes: int32 [4096, 2], P(('sp', 'tp')), may hold values from 0 to 15, all different within a row; in each aligned block of 128 rows (0 to 127, 128 to 255, ...) at most 32 rows name the same one
- route_weights: float32 [4096, 2], P(('sp', 'tp')), may hold values from 0.1 to 1
- w_gate: bfloat16 [16, 2048, 3584], P('sp', None, 'tp'), may hold values from -0.125 to 0.125
- w_up: bfloat16 [16, 2048, 3584], P('sp', None, 'tp'), may hold values from -0.125 to 0.125
- w_down: bfloat16 [16, 3584, 2048], P('sp', 'tp'), may hold values from -0.09375 to 0.09375
- out_gain: float32 [2048], replicated, may hold values from 0.1 to 1.9
Outputs:
- mixed: bfloat16 [4096, 2048], P(('sp', 'tp'))
Inputs may be any that keep to these rules, and one draw needn't show every extreme that they name: `doc_ids`: document numbers never fall along positions; each document holds 1 to 1024 positions, and one holds exactly 1024. `routes`: each row names 2 different experts; among the rows of one device (aligned blocks of 128 rows) no expert is named more than 32 times, and in some blocks one expert is named exactly 32 times.
All inputs are finite; a program needn't handle non-finite values.
Results may differ from a plain program's by a relative error of at most 0.014.
Values may be sent and summed in bfloat16 or wider, within the bound.
A program may use at most 128 MiB of HBM per device.

v0:
```python
import jax
import jax.numpy as jnp
from jax import lax
from jax.sharding import PartitionSpec as P

HEADS = 8
DK = 128
DR = 64
DV = 128
TOPK = 2
REACH = 4


ROPE_THETA = 500000.0
RESIDUAL_SCALE = 2.0**0.5
NORM_EPSILON = 1e-05


def shifted(value, axis, steps):
    count = lax.axis_size(axis)
    leading, last = (max(0, -steps), min(count, count - steps))
    return lax.ppermute(value, axis, [(source, source + steps) for source in range(leading, last)])


def rotate(values, positions):
    half_width = values.shape[-1] // 2
    frequency = ROPE_THETA ** (-2.0 * jnp.arange(half_width, dtype=jnp.float32) / values.shape[-1])
    angles = positions.astype(jnp.float32)[:, None] * frequency[None, :]
    table_shape = (values.shape[0],) + (1,) * (values.ndim - 2) + (half_width,)
    cosine = jnp.cos(angles).reshape(table_shape)
    sine_part = jnp.sin(angles).reshape(table_shape)
    widened = values.astype(jnp.float32)
    first_half = widened[..., :half_width]
    second = widened[..., half_width:]
    return jnp.concatenate(
        [first_half * cosine - second * sine_part, second * cosine + first_half * sine_part], -1
    )


def layer_norm(values, gain_vec):
    centre = jnp.mean(values, -1, keepdims=True)
    spread = jnp.mean(jnp.square(values - centre), -1, keepdims=True)
    return (values - centre) * lax.rsqrt(spread + NORM_EPSILON) * gain_vec


def per_device(
    latent,
    rotary_key,
    doc_ids,
    queries_content,
    queries_rotary,
    w_key_up,
    w_value_up,
    w_out,
    residual,
    norm_gain,
    routes,
    route_weights,
    w_gate,
    w_up,
    w_down,
    out_gain,
):
    tok_dev = latent.shape[0]
    core_count = lax.axis_size("tp")
    chip_count = lax.axis_size("sp")
    heads_here = HEADS // core_count
    head_index = lax.axis_index("tp")
    sp_index = lax.axis_index("sp")
    key_cols = lax.dynamic_slice_in_dim(w_key_up, head_index * heads_here * DK, heads_here * DK, 1)
    value_cols = lax.dynamic_slice_in_dim(
        w_value_up, head_index * heads_here * DV, heads_here * DV, 1
    )
    own_position = sp_index * tok_dev + jnp.arange(tok_dev, dtype=jnp.int32)
    query_turned = rotate(queries_rotary.reshape(tok_dev, heads_here, DR), own_position).astype(
        jnp.bfloat16
    )
    query_block = queries_content.reshape(tok_dev, heads_here, DK)
    pieces = [(latent, rotary_key, doc_ids)]
    for distance in range(1, REACH + 1):
        pieces.append(shifted((latent, rotary_key, doc_ids), "sp", distance))
    ordered = pieces[::-1]
    key_latent = jnp.concatenate([piece[0] for piece in ordered], 0)
    key_rope = jnp.concatenate([piece[1] for piece in ordered], 0)
    key_doc = jnp.concatenate([piece[2] for piece in ordered], 0)
    key_count = key_latent.shape[0]
    key_position = (sp_index - REACH) * tok_dev + jnp.arange(key_count, dtype=jnp.int32)
    key_content = jnp.dot(key_latent, key_cols, preferred_element_type=jnp.float32).astype(
        jnp.bfloat16
    )
    key_content = key_content.reshape(key_count, heads_here, DK)
    values = jnp.dot(key_latent, value_cols, preferred_element_type=jnp.float32).astype(
        jnp.bfloat16
    )
    values = values.reshape(key_count, heads_here, DV)
    key_turned = rotate(key_rope, key_position).astype(jnp.bfloat16)
    score_scale = (DK + DR) ** (-0.5)
    scores = jnp.einsum(
        "phd,qhd->hpq", query_block, key_content, preferred_element_type=jnp.float32
    )
    scores = scores + jnp.einsum(
        "phd,qd->hpq", query_turned, key_turned, preferred_element_type=jnp.float32
    )
    scores = scores * score_scale
    allowed = (key_position[None, :] <= own_position[:, None]) & (key_position[None, :] >= 0)
    allowed = allowed & (key_doc[None, :] == doc_ids[:, None])
    scores = jnp.where(allowed[None], scores, -jnp.inf)
    row_peak = jnp.max(scores, -1, keepdims=True)
    lifted = jnp.exp(scores - row_peak)
    probability = (lifted / jnp.sum(lifted, -1, keepdims=True)).astype(jnp.bfloat16)
    attended = jnp.einsum("hpq,qhd->phd", probability, values, preferred_element_type=jnp.float32)
    attended = attended.astype(jnp.bfloat16).reshape(tok_dev, heads_here * DV)
    partial_value = jnp.dot(attended, w_out, preferred_element_type=jnp.float32)
    projected = lax.psum_scatter(
        partial_value.astype(jnp.bfloat16).astype(jnp.float32).astype(jnp.bfloat16),
        "tp",
        scatter_dimension=0,
        tiled=True,
    ).astype(jnp.float32)
    normed = layer_norm(
        RESIDUAL_SCALE * residual.astype(jnp.float32) + projected, norm_gain
    ).astype(jnp.bfloat16)
    row_count = normed.shape[0]
    model_width = normed.shape[1]
    capacity = max(2, 2 * row_count * TOPK // chip_count)
    flat_route = routes.reshape(-1)
    member = (flat_route[:, None] == jnp.arange(chip_count, dtype=jnp.int32)[None, :]).astype(
        jnp.int32
    )
    slot_rank = jnp.sum((jnp.cumsum(member, 0) - member) * member, 1)
    slot_index = flat_route * capacity + slot_rank
    placing = (
        slot_index[None, :] == jnp.arange(chip_count * capacity, dtype=jnp.int32)[:, None]
    ).astype(jnp.int32)
    placing = jnp.sum(placing.reshape(chip_count * capacity, row_count, TOPK), -1).astype(
        jnp.bfloat16
    )
    outbound = jnp.dot(placing, normed, preferred_element_type=jnp.float32).astype(jnp.bfloat16)
    outbound = outbound.reshape(chip_count, capacity, model_width)
    landed = lax.all_to_all(outbound, "sp", split_axis=0, concat_axis=0, tiled=True)
    arrived = lax.all_gather(landed[:, None], "tp", axis=1, tiled=True)
    flat_rows = arrived.reshape(-1, model_width)
    gate_pre = jnp.dot(flat_rows, w_gate[0], preferred_element_type=jnp.float32)
    upward = jnp.dot(flat_rows, w_up[0], preferred_element_type=jnp.float32)
    hidden = (jax.nn.silu(gate_pre) * upward).astype(jnp.bfloat16)
    partial_value = jnp.dot(hidden, w_down[0], preferred_element_type=jnp.float32)
    partial_value = (
        partial_value.astype(jnp.bfloat16)
        .astype(jnp.float32)
        .reshape(chip_count, core_count, capacity, model_width)
    )
    reduced = lax.psum_scatter(
        partial_value.astype(jnp.bfloat16), "tp", scatter_dimension=1, tiled=True
    )
    returned = lax.all_to_all(
        reduced.reshape(chip_count, capacity, model_width),
        "sp",
        split_axis=0,
        concat_axis=0,
        tiled=True,
    )
    returned = returned.reshape(chip_count * capacity, model_width)
    picked = (
        jnp.take(returned, slot_index, axis=0)
        .reshape(row_count, TOPK, model_width)
        .astype(jnp.float32)
    )
    routed_sum = jnp.sum(picked * route_weights[:, :, None], 1)
    combined = RESIDUAL_SCALE * normed.astype(jnp.float32) + routed_sum
    return layer_norm(combined, out_gain).astype(jnp.bfloat16)


def solution(mesh):
    return jax.shard_map(
        per_device,
        mesh=mesh,
        in_specs=(
            P("sp", None),
            P("sp", None),
            P("sp"),
            P("sp", "tp"),
            P("sp", "tp"),
            P(),
            P(),
            P("tp", None),
            P(("sp", "tp"), None),
            P(),
            P(("sp", "tp"), None),
            P(("sp", "tp"), None),
            P("sp", None, "tp"),
            P("sp", None, "tp"),
            P("sp", "tp", None),
            P(),
        ),
        out_specs=P(("sp", "tp"), None),
        check_vma=False,
    )
```

profile of v0, /device:TPU:16, one launch (start us, length us, event | category | flops | bytes accessed | tf_op | source)
XLA Modules:
  0.0 322.2 jit_solution(12835083971645171798)
XLA Ops:
  6.5 3.6 %collective-permute-start = (bf16[256,256]{1,0:T(8,128)(2,1)}, bf16[256,256]{1,0:T(8,128)(2,1)S(1)}, u32[]{:S(2)}, u32[]{:S(2)}) collective-permute-start(bf16[256,256]{1,0:T(8,128)(2,1)} %param.16), channel_id=1, source_target_pairs={{0,8},{2,10},{4,12},{6,14},{8,16},{10,18},{12,20},{14,22},{16,24},... | collective-permute-start | bytes 393224 | tf_op jit(solution)/shard_map/ppermute | solution.py:22
  10.2 4.4 %collective-permute-start.1 = (bf16[256,256]{1,0:T(8,128)(2,1)}, bf16[256,256]{1,0:T(8,128)(2,1)S(1)}, u32[]{:S(2)}, u32[]{:S(2)}) collective-permute-start(bf16[256,256]{1,0:T(8,128)(2,1)} %param.16), channel_id=1, source_target_pairs={{0,6},{2,8},{4,10},{6,12},{8,14},{10,16},{12,18},{14,20},{16,22},{... | collective-permute-start | bytes 393224 | tf_op jit(solution)/shard_map/ppermute | solution.py:22
  14.5 1.9 collective-permute-start.2
  16.5 2.5 collective-permute-start.3
  18.9 1.9 collective-permute-start.4
  20.9 1.0 copy.54
  22.2 2.4 collective-permute-done.4
  24.6 3.7 %collective-permute-start.5 = (s32[256]{0:T(256)}, s32[256]{0:T(256)S(1)}, u32[]{:S(2)}, u32[]{:S(2)}) collective-permute-start(s32[256]{0:T(256)} %param.18), channel_id=1, source_target_pairs={{0,6},{2,8},{4,10},{6,12},{8,14},{10,16},{12,18},{14,20},{16,22},{... | collective-permute-start | bytes 3080 | tf_op jit(solution)/shard_map/ppermute | solution.py:22
  28.3 3.7 %collective-permute-done.5 = s32[256]{0:T(256)S(1)} collective-permute-done((s32[256]{0:T(256)}, s32[256]{0:T(256)S(1)}, u32[]{:S(2)}, u32[]{:S(2)}) %collective-permute-start.5) | collective-permute-done | bytes 1056 | tf_op jit(solution)/shard_map/ppermute | solution.py:22
  32.1 1.9 collective-permute-start.6
  34.0 4.6 %collective-permute-done.6 = s32[256]{0:T(256)S(1)} collective-permute-done((s32[256]{0:T(256)}, s32[256]{0:T(256)S(1)}, u32[]{:S(2)}, u32[]{:S(2)}) %collective-permute-start.6) | collective-permute-done | bytes 1056 | tf_op jit(solution)/shard_map/ppermute | solution.py:22
  38.7 4.3 %collective-permute-start.7 = (s32[256]{0:T(256)}, s32[256]{0:T(256)S(1)}, u32[]{:S(2)}, u32[]{:S(2)}) collective-permute-start(s32[256]{0:T(256)} %param.18), channel_id=1, source_target_pairs={{0,2},{2,4},{4,6},{6,8},{8,10},{10,12},{12,14},{14,16},{16,18},{18... | collective-permute-start | bytes 3080 | tf_op jit(solution)/shard_map/ppermute | solution.py:22
  42.9 3.2 collective-permute-done.7
  46.1 1.9 collective-permute-start.8
  48.7 1.7 compare_and_fusion
  50.5 1.7 collective-permute-done.8
  52.1 1.9 collective-permute-start.9
  54.1 5.0 %collective-permute-done.9 = bf16[256,64]{0,1:T(8,128)(2,1)S(1)} collective-permute-done((bf16[256,64]{0,1:T(8,128)(2,1)}, bf16[256,64]{0,1:T(8,128)(2,1)S(1)}, u32[]{:S(2)}, u32[]{:S(2)}) %collective-permute-start.9) | collective-permute-done | bytes 32800 | tf_op jit(solution)/shard_map/ppermute | solution.py:22
  59.0 2.4 collective-permute-start.10
  61.4 4.5 %collective-permute-done.10 = bf16[256,64]{0,1:T(8,128)(2,1)S(1)} collective-permute-done((bf16[256,64]{0,1:T(8,128)(2,1)}, bf16[256,64]{0,1:T(8,128)(2,1)S(1)}, u32[]{:S(2)}, u32[]{:S(2)}) %collective-permute-start.10) | collective-permute-done | bytes 32800 | tf_op jit(solution)/shard_map/ppermute | solution.py:22
  65.9 3.4 %collective-permute-start.11 = (bf16[256,64]{0,1:T(8,128)(2,1)}, bf16[256,64]{0,1:T(8,128)(2,1)S(1)}, u32[]{:S(2)}, u32[]{:S(2)}) collective-permute-start(bf16[256,64]{0,1:T(8,128)(2,1)} %param.17), channel_id=1, source_target_pairs={{0,2},{2,4},{4,6},{6,8},{8,10},{10,12},{12,14},{14,16},{16,18},{18... | collective-permute-start | bytes 98312 | tf_op jit(solution)/shard_map/ppermute | solution.py:22
  69.3 4.4 %collective-permute-done.11 = bf16[256,64]{0,1:T(8,128)(2,1)S(1)} collective-permute-done((bf16[256,64]{0,1:T(8,128)(2,1)}, bf16[256,64]{0,1:T(8,128)(2,1)S(1)}, u32[]{:S(2)}, u32[]{:S(2)}) %collective-permute-start.11) | collective-permute-done | bytes 32800 | tf_op jit(solution)/shard_map/ppermute | solution.py:22
  73.8 0.8 constant_dynamic-update-slice_fusion.6
  75.3 0.9 constant_dynamic-update-slice_fusion
  76.3 1.5 convolution_convert_fusion.1
  77.8 0.9 fusion.19
  78.7 1.0 fusion.9
  79.7 2.3 copy-done.2
  82.0 1.0 exponential_reduce_fusion
  83.7 6.2 %fusion.16 = bf16[4,128,256]{2,1,0:T(8,128)(2,1)} fusion(bf16[1280,4,128]{0,2,1:T(8,128)(2,1)S(1)} %bitcast.94, f32[4,256]{1,0:T(4,128)S(1)} %exponential_reduce_fusion, f32[4,256,1280]{1,2,0:T(8,128)} %copy-done.2), kind=kOutput, calls=%fused_computation.25 | convolution fusion | flops 339609856 | bytes 6819840 | tf_op jit(solution)/shard_map/hpq,qhd->phd/dot_general | solution.py:111
  89.9 2.7 convolution_convert_fusion.3
  94.3 5.4 %reduce-scatter.5.cloned.1.call-done = bf16[128,2048]{1,0:T(8,128)(2,1)} async-done(((bf16[256,2048]{1,0:T(8,128)(2,1)}), bf16[128,2048]{1,0:T(8,128)(2,1)}) %reduce-scatter.5.cloned.1.call-update) | async-done | bytes 524304 | tf_op jit(solution)/shard_map/reduce_scatter | solution.py:114
  99.7 1.3 fusion.17
  101.0 1.4 multiply_reduce_fusion.2
  102.4 1.3 multiply_convert_fusion.2
  103.7 0.7 convolution_convert_fusion
  104.4 54.0 %all_to_all.10 = bf16[16,32,2048]{2,1,0:T(8,128)(2,1)} all-to-all(bf16[16,32,2048]{2,1,0:T(8,128)(2,1)S(1)} %bitcast.91), channel_id=1, replica_groups=mesh['sp'=16,'tp'=2] {'sp'}, dimensions={0} | all-to-all | bytes 4194304 | tf_op jit(solution)/shard_map/all_to_all | solution.py:140
  158.6 13.8 %all-gather.3.cloned.1.call-done = bf16[16,64,2048]{2,1,0:T(8,128)(2,1)} async-done(((bf16[16,32,2048]{2,1,0:T(8,128)(2,1)}), bf16[16,64,2048]{2,1,0:T(8,128)(2,1)}) %all-gather.3.cloned.1.call-update) | async-done | bytes 4194320 | tf_op jit(solution)/shard_map/all_gather | solution.py:141
  172.4 13.5 %fusion.5 = f32[1024,1792]{1,0:T(8,128)} fusion(bf16[1024,2048]{1,0:T(8,128)(2,1)} %bitcast.99, bf16[1,2048,1792]{2,1,0:T(8,128)(2,1)} %param.28), kind=kOutput, calls=%fused_computation.6 | convolution fusion | flops 7516192768 | bytes 18874368 | tf_op jit(solution)/shard_map/dot_general | solution.py:143
  185.9 25.8 %fusion.12 = bf16[1024,2048]{1,0:T(8,128)(2,1)} fusion(bf16[1,1792,2048]{2,1,0:T(8,128)(2,1)} %param.30, f32[1024,1792]{1,0:T(8,128)} %fusion.5, bf16[1024,2048]{1,0:T(8,128)(2,1)} %bitcast.100, bf16[1,2048,1792]{2,1,0:T(8,128)(2,1)} %param.29), kind=kOutput, calls=%fused_computation.15 | convolution fusion | flops 15045492736 | bytes 30408704 | tf_op jit(solution)/shard_map/dot_general | solution.py:146
  212.4 28.8 %all-reduce.3.cloned.1.call-done = bf16[16,2,32,2048]{3,2,1,0:T(8,128)(2,1)} async-done(((bf16[16,2,32,2048]{3,2,1,0:T(8,128)(2,1)}), bf16[16,2,32,2048]{3,2,1,0:T(8,128)(2,1)}) %all-reduce.3.cloned.1.call-update) | async-done | bytes 4194320
  241.2 3.8 %dynamic-slice_bitcast_fusion = bf16[16,32,2048]{2,1,0:T(8,128)(2,1)} fusion(bf16[16,2,32,2048]{3,2,1,0:T(8,128)(2,1)} %all-reduce.3.cloned.1.call-done, u32[]{:T(128)} %bitcast.26), kind=kLoop, calls=%fused_computation.21 | loop fusion | bytes 4194308 | tf_op jit(solution)/shard_map/reshape | solution.py:156
  245.0 7.0 %all-to-all-start.1 = ((bf16[16,32,2048]{2,1,0:T(8,128)(2,1)}), bf16[16,32,2048]{2,1,0:T(8,128)(2,1)}, u32[]{:S(2)}, u32[]{:S(2)}) async-start(bf16[16,32,2048]{2,1,0:T(8,128)(2,1)} %dynamic-slice_bitcast_fusion), calls=%async_computation.2 | async-start | bytes 4194304 | tf_op jit(solution)/shard_map/all_to_all | solution.py:155
  252.5 48.1 %all-to-all-done.1 = bf16[16,32,2048]{2,1,0:T(8,128)(2,1)} async-done(((bf16[16,32,2048]{2,1,0:T(8,128)(2,1)}), bf16[16,32,2048]{2,1,0:T(8,128)(2,1)}, u32[]{:S(2)}, u32[]{:S(2)}) %all-to-all-start.1) | async-done | bytes 2097184 | tf_op jit(solution)/shard_map/all_to_all | solution.py:155
  300.6 5.4 %gather_fusion = bf16[256,2048]{1,0:T(8,128)(2,1)} fusion(bf16[512,2048]{1,0:T(8,128)(2,1)} %bitcast.16, s32[1024]{0:T(1024)S(1)} %pad_clamp_fusion), kind=kCustom, calls=%fused_computation | custom fusion | bytes 2098176 | tf_op jit(solution)/shard_map/jit(_take)/gather | solution.py:164
  305.9 2.6 gather.7
  308.5 5.5 %multiply_reduce_fusion = f32[128,2048]{1,0:T(8,128)S(1)} fusion(bf16[128,2,2048]{2,1,0:T(2,128)(2,1)} %gather.7, pred[128,2]{1,0:T(8,128)(4,1)S(1)} %copy.60, f32[128,2]{1,0:T(8,128)S(1)} %copy.62), kind=kLoop, calls=%fused_computation.22 | loop fusion | flops 1835008 | bytes 2098432 | tf_op jit(solution)/shard_map/reduce_sum | solution.py:168
  314.6 1.1 multiply_convert_fusion.1
  (83 shorter events, 6.0 us)
Async XLA Ops:
  6.5 83.3 %copy-start = (bf16[512,2048]{1,0:T(8,128)(2,1)S(1)}, bf16[512,2048]{1,0:T(8,128)(2,1)}, u32[]{:S(2)}) copy-start(bf16[512,2048]{1,0:T(8,128)(2,1)} %param.23) | copy-start | bytes 6291460
  6.5 71.2 %copy-start.4 = (bf16[256,512]{1,0:T(8,128)(2,1)S(1)}, bf16[256,512]{1,0:T(8,128)(2,1)}, u32[]{:S(2)}) copy-start(bf16[256,512]{1,0:T(8,128)(2,1)} %param.19) | copy-start | bytes 786436
  6.5 93.1 %reduce-scatter.5.cloned.1.call-start = ((), (), s32[]{:S(2)}) async-start(), calls=%async_computation.3 | async-start | bytes 1572864 | tf_op jit(solution)/shard_map/reduce_scatter | solution.py:114
  6.5 68.7 %collective-permute-start = (bf16[256,256]{1,0:T(8,128)(2,1)}, bf16[256,256]{1,0:T(8,128)(2,1)S(1)}, u32[]{:S(2)}, u32[]{:S(2)}) collective-permute-start(bf16[256,256]{1,0:T(8,128)(2,1)} %param.16), channel_id=1, source_target_pairs={{0,8},{2,10},{4,12},{6,14},{8,16},{10,18},{12,20},{14,22},{16,24},... | collective-permute-start | bytes 393224 | tf_op jit(solution)/shard_map/ppermute | solution.py:22
  10.2 65.1 %collective-permute-start.1 = (bf16[256,256]{1,0:T(8,128)(2,1)}, bf16[256,256]{1,0:T(8,128)(2,1)S(1)}, u32[]{:S(2)}, u32[]{:S(2)}) collective-permute-start(bf16[256,256]{1,0:T(8,128)(2,1)} %param.16), channel_id=1, source_target_pairs={{0,6},{2,8},{4,10},{6,12},{8,14},{10,16},{12,18},{14,20},{16,22},{... | collective-permute-start | bytes 393224 | tf_op jit(solution)/shard_map/ppermute | solution.py:22
  14.5 60.8 %collective-permute-start.2 = (bf16[256,256]{1,0:T(8,128)(2,1)}, bf16[256,256]{1,0:T(8,128)(2,1)S(1)}, u32[]{:S(2)}, u32[]{:S(2)}) collective-permute-start(bf16[256,256]{1,0:T(8,128)(2,1)} %param.16), channel_id=1, source_target_pairs={{0,4},{2,6},{4,8},{6,10},{8,12},{10,14},{12,16},{14,18},{16,20},{1... | collective-permute-start | bytes 393224 | tf_op jit(solution)/shard_map/ppermute | solution.py:22
  16.5 58.9 %collective-permute-start.3 = (bf16[256,256]{1,0:T(8,128)(2,1)}, bf16[256,256]{1,0:T(8,128)(2,1)S(1)}, u32[]{:S(2)}, u32[]{:S(2)}) collective-permute-start(bf16[256,256]{1,0:T(8,128)(2,1)} %param.16), channel_id=1, source_target_pairs={{0,2},{2,4},{4,6},{6,8},{8,10},{10,12},{12,14},{14,16},{16,18},{18... | collective-permute-start | bytes 393224 | tf_op jit(solution)/shard_map/ppermute | solution.py:22
  18.9 5.7 %collective-permute-start.4 = (s32[256]{0:T(256)}, s32[256]{0:T(256)S(1)}, u32[]{:S(2)}, u32[]{:S(2)}) collective-permute-start(s32[256]{0:T(256)} %param.18), channel_id=1, source_target_pairs={{0,8},{2,10},{4,12},{6,14},{8,16},{10,18},{12,20},{14,22},{16,24},... | collective-permute-start | bytes 3080 | tf_op jit(solution)/shard_map/ppermute | solution.py:22
  24.6 7.5 %collective-permute-start.5 = (s32[256]{0:T(256)}, s32[256]{0:T(256)S(1)}, u32[]{:S(2)}, u32[]{:S(2)}) collective-permute-start(s32[256]{0:T(256)} %param.18), channel_id=1, source_target_pairs={{0,6},{2,8},{4,10},{6,12},{8,14},{10,16},{12,18},{14,20},{16,22},{... | collective-permute-start | bytes 3080 | tf_op jit(solution)/shard_map/ppermute | solution.py:22
  32.1 6.6 %collective-permute-start.6 = (s32[256]{0:T(256)}, s32[256]{0:T(256)S(1)}, u32[]{:S(2)}, u32[]{:S(2)}) collective-permute-start(s32[256]{0:T(256)} %param.18), channel_id=1, source_target_pairs={{0,4},{2,6},{4,8},{6,10},{8,12},{10,14},{12,16},{14,18},{16,20},{1... | collective-permute-start | bytes 3080 | tf_op jit(solution)/shard_map/ppermute | solution.py:22
  38.7 7.5 %collective-permute-start.7 = (s32[256]{0:T(256)}, s32[256]{0:T(256)S(1)}, u32[]{:S(2)}, u32[]{:S(2)}) collective-permute-start(s32[256]{0:T(256)} %param.18), channel_id=1, source_target_pairs={{0,2},{2,4},{4,6},{6,8},{8,10},{10,12},{12,14},{14,16},{16,18},{18... | collective-permute-start | bytes 3080 | tf_op jit(solution)/shard_map/ppermute | solution.py:22
  46.1 6.0 %collective-permute-start.8 = (bf16[256,64]{0,1:T(8,128)(2,1)}, bf16[256,64]{0,1:T(8,128)(2,1)S(1)}, u32[]{:S(2)}, u32[]{:S(2)}) collective-permute-start(bf16[256,64]{0,1:T(8,128)(2,1)} %param.17), channel_id=1, source_target_pairs={{0,8},{2,10},{4,12},{6,14},{8,16},{10,18},{12,20},{14,22},{16,24},... | collective-permute-start | bytes 98312 | tf_op jit(solution)/shard_map/ppermute | solution.py:22
  52.1 6.9 %collective-permute-start.9 = (bf16[256,64]{0,1:T(8,128)(2,1)}, bf16[256,64]{0,1:T(8,128)(2,1)S(1)}, u32[]{:S(2)}, u32[]{:S(2)}) collective-permute-start(bf16[256,64]{0,1:T(8,128)(2,1)} %param.17), channel_id=1, source_target_pairs={{0,6},{2,8},{4,10},{6,12},{8,14},{10,16},{12,18},{14,20},{16,22},{... | collective-permute-start | bytes 98312 | tf_op jit(solution)/shard_map/ppermute | solution.py:22
  59.0 6.9 %collective-permute-start.10 = (bf16[256,64]{0,1:T(8,128)(2,1)}, bf16[256,64]{0,1:T(8,128)(2,1)S(1)}, u32[]{:S(2)}, u32[]{:S(2)}) collective-permute-start(bf16[256,64]{0,1:T(8,128)(2,1)} %param.17), channel_id=1, source_target_pairs={{0,4},{2,6},{4,8},{6,10},{8,12},{10,14},{12,16},{14,18},{16,20},{1... | collective-permute-start | bytes 98312 | tf_op jit(solution)/shard_map/ppermute | solution.py:22
  65.9 7.8 %collective-permute-start.11 = (bf16[256,64]{0,1:T(8,128)(2,1)}, bf16[256,64]{0,1:T(8,128)(2,1)S(1)}, u32[]{:S(2)}, u32[]{:S(2)}) collective-permute-start(bf16[256,64]{0,1:T(8,128)(2,1)} %param.17), channel_id=1, source_target_pairs={{0,2},{2,4},{4,6},{6,8},{8,10},{10,12},{12,14},{14,16},{16,18},{18... | collective-permute-start | bytes 98312 | tf_op jit(solution)/shard_map/ppermute | solution.py:22
  79.7 2.3 copy-start.2
  82.0 1.0 copy-start.5
  83.6 9.0 %copy-start.6 = (s32[128,2]{0,1:T(2,128)S(1)}, s32[128,2]{0,1:T(2,128)}, u32[]{:S(2)}) copy-start(s32[128,2]{0,1:T(2,128)} %param.26) | copy-start | bytes 3076
  89.9 9.8 %copy-start.3 = (bf16[128,2048]{1,0:T(8,128)(2,1)S(1)}, bf16[128,2048]{1,0:T(8,128)(2,1)}, u32[]{:S(2)}) copy-start(bf16[128,2048]{1,0:T(8,128)(2,1)} %param.24) | copy-start | bytes 1572868
  89.9 12.5 %copy-start.7 = (f32[2048]{0:T(1024)S(1)}, f32[2048]{0:T(1024)}, u32[]{:S(2)}) copy-start(f32[2048]{0:T(1024)} %param.25) | copy-start | bytes 24580
  92.6 79.8 %all-gather.3.cloned.1.call-start = ((), (), s32[]{:S(2)}) async-start(), calls=%async_computation.4 | async-start | bytes 6291456 | tf_op jit(solution)/shard_map/all_gather | solution.py:141
  158.4 82.8 %all-reduce.3.cloned.1.call-start = ((), (), s32[]{:S(2)}) async-start(), calls=%async_computation.5 | async-start | bytes 8388608
  185.9 25.9 %copy-start.10 = (u32[32]{0:T(128)S(1)}, u32[32]{0:T(128)}, u32[]{:S(2)}) copy-start(u32[32]{0:T(128)} %constant.72) | copy-start | bytes 388
  211.8 40.6 %copy-start.9 = (f32[128,2]{0,1:T(2,128)S(1)}, f32[128,2]{0,1:T(2,128)}, u32[]{:S(2)}) copy-start(f32[128,2]{0,1:T(2,128)} %param.27) | copy-start | bytes 3076
  245.0 55.6 %all-to-all-start.1 = ((bf16[16,32,2048]{2,1,0:T(8,128)(2,1)}), bf16[16,32,2048]{2,1,0:T(8,128)(2,1)}, u32[]{:S(2)}, u32[]{:S(2)}) async-start(bf16[16,32,2048]{2,1,0:T(8,128)(2,1)} %dynamic-slice_bitcast_fusion), calls=%async_computation.2 | async-start | bytes 4194304 | tf_op jit(solution)/shard_map/all_to_all | solution.py:155
  300.6 15.0 %copy-start.1 = (bf16[512,2048]{1,0:T(8,128)(2,1)S(1)}, bf16[512,2048]{1,0:T(8,128)(2,1)}, u32[]{:S(2)}) copy-start(bf16[512,2048]{1,0:T(8,128)(2,1)} %param.23) | copy-start | bytes 6291460
  305.9 8.6 %copy-start.8 = (f32[2048]{0:T(1024)S(1)}, f32[2048]{0:T(1024)}, u32[]{:S(2)}) copy-start(f32[2048]{0:T(1024)} %param.31) | copy-start | bytes 24580
Sparse Core Ops, SparseCore 0:
  92.8 6.8 reduce-scatter.4
  158.5 13.8 all-gather.2
  211.9 29.2 all-reduce.2
where the time goes:
time: 323 us; the launch traced here: 322 us
  waiting for transfers between devices  126 us (39%)
  blocking collectives  54 us (17%)
  matrix products  52.9 us (16%)
  starting transfers between devices  40.9 us (13%)
  local copies, waits for them, and re-layouts  19.4 us (6%)
  other arithmetic  15.7 us (5%)
  between operations  13.6 us (4%)
    all_to_all x1, blocking collectives, per_device(): lax.all_to_all(outbound, 'sp', split_axis=0, concat_axis=0, tiled=True)  54 us
    all_to_all x1, waiting for transfers between devices, per_device(): lax.all_to_all(reduced.reshape(chip_count, capacity, model_width), 'sp',...  48.1 us
    ppermute x12, starting transfers between devices, shifted(): lax.ppermute(value, axis, [(source, source + steps) for source in range(l...  33.7 us
    ppermute x12, waiting for transfers between devices, shifted(): lax.ppermute(value, axis, [(source, source + steps) for source in range(l...  29.6 us
    unnamed x4, waiting for transfers between devices  28.9 us
    dot_general x1, matrix products, per_device(): jnp.dot(hidden, w_down[0], preferred_element_type=jnp.float32)  25.8 us
    all_gather x1, waiting for transfers between devices, per_device(): arrived = lax.all_gather(landed[:, None], 'tp', axis=1, tiled=True)  13.8 us
    dot_general x1, matrix products, per_device(): gate_pre = jnp.dot(flat_rows, w_gate[0], preferred_element_type=jnp.float32)  13.5 us
  transfers between devices with their start and end apart: 16, of which 12 were waited for; matrix products, arithmetic and copies ran while one was open for 2% of the time, Pallas kernels for 0%

commit v1 on v0

v1 whole, which is shorter than its diff:
```python
import functools

import jax
import jax.numpy as jnp
from jax import lax
from jax.experimental import pallas as pl
from jax.experimental.pallas import tpu as pltpu
from jax.sharding import PartitionSpec as P

HEADS = 8
DK = 128
DR = 64
DV = 128
TOPK = 2
REACH = 4
CHUNKS = 4


ROPE_THETA = 500000.0
RESIDUAL_SCALE = 2.0**0.5
NORM_EPSILON = 1e-05
MESH = pl.DeviceIdType.MESH
VMEM = pl.BlockSpec(memory_space=pltpu.VMEM)
ANY = pl.BlockSpec(memory_space=pl.ANY)
F32 = jnp.float32
BF16 = jnp.bfloat16


def rotate(values, positions):
    half_width = values.shape[-1] // 2
    frequency = ROPE_THETA ** (-2.0 * jnp.arange(half_width, dtype=jnp.float32) / values.shape[-1])
    angles = positions.astype(jnp.float32)[:, None] * frequency[None, :]
    table_shape = (values.shape[0],) + (1,) * (values.ndim - 2) + (half_width,)
    cosine = jnp.cos(angles).reshape(table_shape)
    sine_part = jnp.sin(angles).reshape(table_shape)
    widened = values.astype(jnp.float32)
    first_half = widened[..., :half_width]
    second = widened[..., half_width:]
    return jnp.concatenate(
        [first_half * cosine - second * sine_part, second * cosine + first_half * sine_part], -1
    )


def layer_norm(values, gain_vec):
    centre = jnp.mean(values, -1, keepdims=True)
    spread = jnp.mean(jnp.square(values - centre), -1, keepdims=True)
    return (values - centre) * lax.rsqrt(spread + NORM_EPSILON) * gain_vec


def dot(a, b):
    return jnp.dot(a, b, preferred_element_type=F32)


def dot_nt(a, b):
    return lax.dot_general(a, b, (((1,), (1,)), ((), ())), preferred_element_type=F32)


def remote(src, dst, send_sem, recv_sem, sp, tp):
    return pltpu.make_async_remote_copy(
        src_ref=src, dst_ref=dst, send_sem=send_sem, recv_sem=recv_sem,
        device_id=(sp, tp), device_id_type=MESH,
    )


def greet(devices):
    barrier = pltpu.get_barrier_semaphore()
    for device in devices:
        pl.semaphore_signal(barrier, inc=1, device_id=device, device_id_type=MESH)
    pl.semaphore_wait(barrier, len(devices))


def attention_kernel(
    n, pack_ref, q_ref, hot_ref, wk_ref, wv_ref, wo_ref, res_ref, gain_ref, out_ref,
    held, wo_other, scores, vals, att, att_other, send_sem, recv_sem, wo_sem, att_sem,
):
    me, tp = lax.axis_index("sp"), lax.axis_index("tp")
    tok = pack_ref.shape[0]
    rank = wk_ref.shape[0]
    heads = q_ref.shape[0]
    rows = out_ref.shape[0]
    mine = (me, tp)
    del mine
    greet(
        [(lax.rem(me + d, n), tp) for d in range(1, REACH + 1)]
        + [(lax.rem(me + n - d, n), tp) for d in range(1, REACH + 1)]
        + [(me, 1 - tp)]
    )
    copies = [None]
    for d in range(1, REACH + 1):
        copies.append(
            remote(pack_ref, held.at[d - 1], send_sem.at[d - 1], recv_sem.at[d - 1],
                   lax.rem(me + d, n), tp)
        )
        copies[d].start()
    share = remote(wo_ref, wo_other, wo_sem.at[0], wo_sem.at[1], me, 1 - tp)
    share.start()
    key_cols = pl.ds(pl.multiple_of(tp * heads * DK, 128), heads * DK)
    value_cols = pl.ds(pl.multiple_of(tp * heads * DV, 128), heads * DV)
    wk = wk_ref[:, key_cols]
    wv = wv_ref[:, value_cols]
    hot = hot_ref[...]
    for d in range(REACH + 1):
        if d == 0:
            block = pack_ref[...]
        else:
            copies[d].wait_recv()
            block = held[d - 1]
        span = slice((REACH - d) * tok, (REACH - d + 1) * tok)
        lat, tail = block[:, :rank], block[:, rank:]
        kc = dot(lat, wk).astype(BF16)
        vals[span, :] = dot(lat, wv).astype(BF16)
        allowed = dot_nt(hot, tail) > 0.5
        q_at = lax.broadcasted_iota(jnp.int32, (tok, tok), 0)
        k_at = lax.broadcasted_iota(jnp.int32, (tok, tok), 1) - d * tok
        allowed = allowed & (k_at <= q_at) & (k_at + me * tok >= 0)
        for h in range(heads):
            key = jnp.concatenate([kc[:, h * DK:(h + 1) * DK], tail], 1)
            s = dot_nt(q_ref[h], key) * ((DK + DR) ** (-0.5))
            scores[h, :, span] = jnp.where(allowed, s, -jnp.inf)
    for h in range(heads):
        s = scores[h]
        lifted = jnp.exp(s - jnp.max(s, -1, keepdims=True))
        prob = (lifted * (1.0 / jnp.sum(lifted, -1, keepdims=True))).astype(BF16)
        att[:, h * DV:(h + 1) * DV] = dot(prob, vals[:, h * DV:(h + 1) * DV]).astype(BF16)
    theirs = pl.ds(pl.multiple_of((1 - tp) * rows, rows), rows)
    ours = pl.ds(pl.multiple_of(tp * rows, rows), rows)
    swap = remote(att.at[theirs], att_other, att_sem.at[0], att_sem.at[1], me, 1 - tp)
    swap.start()
    projected = dot(att[ours, :], wo_ref[...]).astype(BF16).astype(F32)
    share.wait_recv()
    swap.wait_recv()
    projected = projected + dot(att_other[...], wo_other[...]).astype(BF16).astype(F32)
    total = RESIDUAL_SCALE * res_ref[...].astype(F32) + projected
    out_ref[...] = layer_norm(total, gain_ref[...]).astype(BF16)
    for d in range(1, REACH + 1):
        copies[d].wait_send()
    share.wait_send()
    swap.wait_send()


def attention(n, pack, q, hot, wk, wv, wo, res, gain):
    tok, wide = pack.shape
    heads = q.shape[0]
    rows, width = res.shape
    return pl.pallas_call(
        functools.partial(attention_kernel, n),
        out_shape=jax.ShapeDtypeStruct((rows, width), BF16),
        in_specs=[VMEM] * 8,
        out_specs=VMEM,
        scratch_shapes=[
            pltpu.VMEM((REACH, tok, wide), BF16),
            pltpu.VMEM(wo.shape, BF16),
            pltpu.VMEM((heads, tok, (REACH + 1) * tok), F32),
            pltpu.VMEM(((REACH + 1) * tok, heads * DV), BF16),
            pltpu.VMEM((tok, heads * DV), BF16),
            pltpu.VMEM((rows, heads * DV), BF16),
            pltpu.SemaphoreType.DMA((REACH,)),
            pltpu.SemaphoreType.DMA((REACH,)),
            pltpu.SemaphoreType.DMA((2,)),
            pltpu.SemaphoreType.DMA((2,)),
        ],
        compiler_params=pltpu.CompilerParams(
            collective_id=0, has_side_effects=True, vmem_limit_bytes=40 * 2**20
        ),
        name="attention",
    )(pack, q, hot, wk, wv, wo, res, gain)


def expert_kernel(
    n, cap, normed_ref, placing_ref, pick_ref, weight_ref, gain_ref, wg_hbm, wu_hbm, wd_hbm, out_ref,
    wg, wu, wd, outb, xin, hid, part, recvp, result, returned, total,
    w_sem, send_sem, recv_sem, fsend_sem, frecv_sem, psend_sem, precv_sem, rsend_sem, rrecv_sem,
):
    me, tp = lax.axis_index("sp"), lax.axis_index("tp")
    width = normed_ref.shape[1]
    hidden = hid.shape[1]
    per = n // CHUNKS
    tall = per * 2 * cap
    loads = [
        pltpu.make_async_copy(src, dst, w_sem.at[i])
        for i, (src, dst) in enumerate(((wg_hbm, wg), (wu_hbm, wu), (wd_hbm, wd)))
    ]
    for load in loads:
        load.start()
    normed = normed_ref[...]
    for c in range(CHUNKS):
        lines = slice(c * per * cap, (c + 1) * per * cap)
        outb[c * per:(c + 1) * per] = (
            dot(placing_ref[lines, :], normed).astype(BF16).reshape(per, cap, width)
        )
    greet([(lax.rem(me + d, n), tp) for d in range(1, n)] + [(me, 1 - tp)])
    sends, forwards, parts, returns = [None], [], [], [None]
    for d in range(1, n):
        to = lax.rem(me + d, n)
        sends.append(remote(outb.at[to], xin.at[d, tp], send_sem.at[d], recv_sem.at[d], to, tp))
        sends[d].start()
    xin[0, tp] = outb[me]
    for d in range(n):
        forwards.append(
            remote(xin.at[d, tp], xin.at[d, tp], fsend_sem.at[d], frecv_sem.at[d], me, 1 - tp)
        )
    for c in range(CHUNKS):
        group = pl.ds(c * per, per)
        parts.append(
            remote(part.at[1 - tp, group], recvp.at[group], psend_sem.at[c], precv_sem.at[c],
                   me, 1 - tp)
        )
    for d in range(1, n):
        back = lax.rem(me + n - d, n)
        returns.append(
            remote(result.at[d], returned.at[me], rsend_sem.at[d], rrecv_sem.at[d], back, tp)
        )

    def finish(c):
        parts[c].wait_recv()
        for d in range(c * per, (c + 1) * per):
            value = (part[tp, d].astype(F32) + recvp[d].astype(F32)).astype(BF16)
            if d == 0:
                returned[me] = value
            else:
                result[d] = value
                returns[d].start()

    step = 256 if hidden % 256 == 0 else 128
    for c in range(CHUNKS):
        group = range(c * per, (c + 1) * per)
        for d in group:
            if d > 0:
                sends[d].wait_recv()
            forwards[d].start()
        if c == 0:
            loads[0].wait()
            loads[1].wait()
        for d in group:
            forwards[d].wait_recv()

        def up(j, carry):
            cols = pl.ds(pl.multiple_of(j * step, step), step)
            x = xin[c * per:(c + 1) * per].reshape(tall, width)
            gate_pre = dot(x, wg[:, cols])
            upward = dot(x, wu[:, cols])
            hid[:, cols] = (gate_pre / (1.0 + jnp.exp(-gate_pre)) * upward).astype(BF16)
            return carry

        lax.fori_loop(0, hidden // step, up, 0)
        if c > 0:
            finish(c - 1)
        if c == 0:
            loads[2].wait()

        def down(j, carry):
            cols = pl.ds(pl.multiple_of(j * 512, 512), 512)
            o = dot(hid[...], wd[:, cols]).astype(BF16).reshape(per, 2, cap, 512)
            for t in range(2):
                part[t, c * per:(c + 1) * per, :, cols] = o[:, t]
            return carry

        lax.fori_loop(0, width // 512, down, 0)
        parts[c].start()
    finish(CHUNKS - 1)
    for d in range(1, n):
        returns[d].wait_recv()
    weights = weight_ref[...]
    for j in range(width // 512):
        cols = slice(j * 512, (j + 1) * 512)
        rows_back = returned[:, :, cols].reshape(n * cap, 512)
        value = RESIDUAL_SCALE * normed_ref[:, cols].astype(F32)
        for k in range(TOPK):
            value = value + weights[:, k:k + 1] * dot(pick_ref[k], rows_back)
        total[:, cols] = value
    out_ref[...] = layer_norm(total[...], gain_ref[...]).astype(BF16)
    for d in range(n):
        forwards[d].wait_send()
        if d > 0:
            sends[d].wait_send()
            returns[d].wait_send()
    for c in range(CHUNKS):
        parts[c].wait_send()


def experts(n, cap, normed, placing, pick, weights, gain, wg, wu, wd):
    rows, width = normed.shape
    hidden = wg.shape[1]
    tall = n // CHUNKS * 2 * cap
    block = (n, cap, width)
    return pl.pallas_call(
        functools.partial(expert_kernel, n, cap),
        out_shape=jax.ShapeDtypeStruct((rows, width), BF16),
        in_specs=[VMEM] * 5 + [ANY] * 3,
        out_specs=VMEM,
        scratch_shapes=[
            pltpu.VMEM(wg.shape, BF16),
            pltpu.VMEM(wu.shape, BF16),
            pltpu.VMEM(wd.shape, BF16),
            pltpu.VMEM(block, BF16),
            pltpu.VMEM((n, 2, cap, width), BF16),
            pltpu.VMEM((tall, hidden), BF16),
            pltpu.VMEM((2,) + block, BF16),
            pltpu.VMEM(block, BF16),
            pltpu.VMEM(block, BF16),
            pltpu.VMEM(block, BF16),
            pltpu.VMEM((rows, width), F32),
            pltpu.SemaphoreType.DMA((3,)),
            pltpu.SemaphoreType.DMA((n,)),
            pltpu.SemaphoreType.DMA((n,)),
            pltpu.SemaphoreType.DMA((n,)),
            pltpu.SemaphoreType.DMA((n,)),
            pltpu.SemaphoreType.DMA((CHUNKS,)),
            pltpu.SemaphoreType.DMA((CHUNKS,)),
            pltpu.SemaphoreType.DMA((n,)),
            pltpu.SemaphoreType.DMA((n,)),
        ],
        compiler_params=pltpu.CompilerParams(
            collective_id=1, has_side_effects=True, vmem_limit_bytes=58 * 2**20
        ),
        name="experts",
    )(normed, placing, pick, weights, gain, wg, wu, wd)


def per_device(
    latent,
    rotary_key,
    doc_ids,
    queries_content,
    queries_rotary,
    w_key_up,
    w_value_up,
    w_out,
    residual,
    norm_gain,
    routes,
    route_weights,
    w_gate,
    w_up,
    w_down,
    out_gain,
):
    tok_dev = latent.shape[0]
    core_count = lax.axis_size("tp")
    chip_count = lax.axis_size("sp")
    heads_here = HEADS // core_count
    sp_index = lax.axis_index("sp")
    own_position = sp_index * tok_dev + jnp.arange(tok_dev, dtype=jnp.int32)
    query_turned = rotate(queries_rotary.reshape(tok_dev, heads_here, DR), own_position).astype(BF16)
    query_block = queries_content.reshape(tok_dev, heads_here, DK)
    q = jnp.concatenate([query_block, query_turned, jnp.zeros_like(query_turned)], -1)
    q = q.transpose(1, 0, 2)
    key_turned = rotate(rotary_key, own_position).astype(BF16)
    hot = (doc_ids[:, None] == jnp.arange(DR, dtype=jnp.int32)[None, :]).astype(BF16)
    pack = jnp.concatenate([latent, key_turned, hot], 1)
    hot = jnp.concatenate([jnp.zeros_like(hot), hot], 1)
    normed = attention(
        chip_count, pack, q, hot, w_key_up, w_value_up, w_out, residual, norm_gain[None]
    )
    row_count = normed.shape[0]
    capacity = max(2, 2 * row_count * TOPK // chip_count)
    flat_route = routes.reshape(-1)
    member = (flat_route[:, None] == jnp.arange(chip_count, dtype=jnp.int32)[None, :]).astype(
        jnp.int32
    )
    slot_rank = jnp.sum((jnp.cumsum(member, 0) - member) * member, 1)
    slot_index = (flat_route * capacity + slot_rank).reshape(row_count, TOPK)
    slots = jnp.arange(chip_count * capacity, dtype=jnp.int32)
    pick = (slot_index.T[:, :, None] == slots).astype(BF16)
    placing = jnp.any(slot_index[None] == slots[:, None, None], -1).astype(BF16)
    return experts(
        chip_count, capacity, normed, placing, pick, route_weights, out_gain[None],
        w_gate[0], w_up[0], w_down[0],
    )


def solution(mesh):
    return jax.shard_map(
        per_device,
        mesh=mesh,
        in_specs=(
            P("sp", None),
            P("sp", None),
            P("sp"),
            P("sp", "tp"),
            P("sp", "tp"),
            P(),
            P(),
            P("tp", None),
            P(("sp", "tp"), None),
            P(),
            P(("sp", "tp"), None),
            P(("sp", "tp"), None),
            P("sp", None, "tp"),
            P("sp", None, "tp"),
            P("sp", "tp", None),
            P(),
        ),
        out_specs=P(("sp", "tp"), None),
        check_vma=False,
    )
```

time: 323 us -> 180 us (0.56)
  the two profiles are of different devices: /device:TPU:16 before, /device:TPU:0 now
where the time goes in v1:
time: 180 us; the launch traced here: 179 us
  Pallas kernels  156 us (87%)
  local copies, waits for them, and re-layouts  14.6 us (8%)
  other arithmetic  8.98 us (5%)
    pallas_call x1, Pallas kernels, experts(): pl.pallas_call(functools.partial(expert_kernel, n, cap), out_shape=jax.Sh...  134 us
    pallas_call x1, Pallas kernels, attention(): pl.pallas_call(functools.partial(attention_kernel, n), out_shape=jax.Shap...  21.5 us
    unnamed x24, local copies, waits for them, and re-layouts  11.3 us

profile of v1, /device:TPU:0, one launch (start us, length us, event | category | flops | bytes accessed | tf_op | source)
XLA Modules:
  0.0 179.3 jit_solution(15246424160477898689)
XLA Ops:
  0.0 0.0 copy-start.5
  0.0 0.0 copy-start.2
  0.0 0.0 copy-start.3
  0.0 0.0 copy-start
  0.0 0.0 copy-start.6
  0.0 0.0 copy-start.7
  0.0 1.0 copy.47
  1.1 1.3 multiply_cosine_fusion
  2.4 1.0 copy.50
  3.4 0.7 fusion.7
  4.1 1.9 %copy.59 = f32[256,4,32]{2,0,1:T(8,128)} copy(f32[256,4,32]{0,2,1:T(8,128)} %get-tuple-element.10) | data formatting | bytes 262144
  6.0 1.0 copy.60
  7.0 2.1 %subtract_convert_fusion = (bf16[256,4,32]{2,0,1:T(8,128)(2,1)S(1)}, bf16[256,4,32]{2,0,1:T(8,128)(2,1)}) fusion(f32[256,4,32]{2,0,1:T(8,128)} %copy.60, f32[256,4,32]{2,0,1:T(8,128)} %copy.59, f32[256,32]{1,0:T(8,128)} %get-tuple-element.12, f32[256,32]{1,0:T(8,128)S(1)} %get-tuple-element.11), kind=kLoop, calls=%fused_computation.4 | loop fusion | flops 262144 | bytes 458752 | tf_op jit(solution)/shard_map/convert.1
  9.0 1.8 copy.49
  10.8 1.8 copy.53
  12.6 0.1 pad.4.clone
  12.7 1.2 maximum_bitcast_fusion.q_ref
  13.9 0.8 fusion.2
  14.7 1.1 pad_maximum_fusion.pack_ref
  15.8 0.1 concatenate.17.hot_ref
  15.9 0.0 copy-done.5
  15.9 0.0 copy-done.2
  15.9 0.0 copy-done.3
  15.9 0.0 copy-done
  15.9 0.0 copy-start.4
  16.0 1.0 copy-done.4
  17.0 21.5 %attention.1.normed_ref = bf16[128,2048]{1,0:T(8,128)(2,1)S(1)} custom-call(bf16[256,384]{1,0:T(8,128)(2,1)S(1)} %pad_maximum_fusion.pack_ref, bf16[4,256,256]{2,1,0:T(8,128)(2,1)S(1)} %maximum_bitcast_fusion.q_ref, bf16[256,128]{1,0:T(8,128)(2,1)S(1)} %concatenate.17.hot_ref, bf16[256,1024]{1,0:T(8,128)(2,1)S(1)} %copy-done.2, ...), custom_call_target="tpu_custom_call" | custom-call | tf_op jit(solution)/shard_map/attention/pallas_call | solution.py:145
  38.5 0.0 copy-start.1
  38.5 0.8 copy-done.1
  39.2 0.0 copy-done.6
  39.3 0.1 copy.54
  39.4 0.1 eq.71
  39.5 0.8 reduce-window.6
  40.3 0.2 slice_reduce_fusion
  40.5 0.1 eq.67
  40.7 0.1 fusion.5
  40.8 0.1 reduce_sum.12
  40.9 0.1 copy.57
  41.0 0.8 fusion.1.pick_ref
  41.8 0.1 fusion
  41.9 0.7 convert_element_type.42.placing_ref
  42.5 0.0 copy-done.7
  42.6 0.7 copy.58.weight_ref
  43.3 134.1 %experts.1 = bf16[128,2048]{1,0:T(8,128)(2,1)} custom-call(bf16[128,2048]{1,0:T(8,128)(2,1)} %copy-done.1, bf16[512,128]{1,0:T(8,128)(2,1)} %convert_element_type.42.placing_ref, bf16[2,128,512]{2,1,0:T(8,128)(2,1)} %fusion.1.pick_ref, f32[128,2]{1,0:T(8,128)} %copy.58.weight_ref, f32[1,2048]{1,0:T(1,128)} %bitcast.37, bf16[2048,1792]{1,0:T(8,128)(2,1)} %bitcast.31, ...), custom_call_target="tpu_custom_call" | custom-call | tf_op jit(solution)/shard_map/experts/pallas_call | solution.py:286
  177.4 1.9 %copy.64 = bf16[128,2048]{1,0:T(8,128)(2,1)} copy(bf16[128,2048]{1,0:T(8,128)(2,1)} %experts.1) | data formatting | bytes 1048576
  (8 shorter events, 0.1 us)
Async XLA Ops:
  0.0 15.9 %copy-start.5 = (f32[2048]{0:T(1024)S(1)}, f32[2048]{0:T(1024)}, u32[]{:S(2)}) copy-start(f32[2048]{0:T(1024)} %param.25) | copy-start | bytes 24580
  0.0 15.9 %copy-start.2 = (bf16[256,1024]{1,0:T(8,128)(2,1)S(1)}, bf16[256,1024]{1,0:T(8,128)(2,1)}, u32[]{:S(2)}) copy-start(bf16[256,1024]{1,0:T(8,128)(2,1)} %wk_ref.1) | copy-start | bytes 1572868
  0.0 15.9 %copy-start.3 = (bf16[256,1024]{1,0:T(8,128)(2,1)S(1)}, bf16[256,1024]{1,0:T(8,128)(2,1)}, u32[]{:S(2)}) copy-start(bf16[256,1024]{1,0:T(8,128)(2,1)} %wv_ref.1) | copy-start | bytes 1572868
  0.0 15.9 %copy-start = (bf16[512,2048]{1,0:T(8,128)(2,1)S(1)}, bf16[512,2048]{1,0:T(8,128)(2,1)}, u32[]{:S(2)}) copy-start(bf16[512,2048]{1,0:T(8,128)(2,1)} %wo_ref.1) | copy-start | bytes 6291460
  0.0 39.2 %copy-start.6 = (s32[128,2]{0,1:T(2,128)S(1)}, s32[128,2]{0,1:T(2,128)}, u32[]{:S(2)}) copy-start(s32[128,2]{0,1:T(2,128)} %param.26) | copy-start | bytes 3076
  0.0 42.5 %copy-start.7 = (f32[128,2]{0,1:T(2,128)S(1)}, f32[128,2]{0,1:T(2,128)}, u32[]{:S(2)}) copy-start(f32[128,2]{0,1:T(2,128)} %param.27) | copy-start | bytes 3076
  15.9 1.0 copy-start.4
  38.5 0.8 copy-start.1

commit v2 on v1

--- a/solution.py
+++ b/solution.py
@@ -7,7 +7,6 @@
 from jax.experimental.pallas import tpu as pltpu
 from jax.sharding import PartitionSpec as P
 
-HEADS = 8
 DK = 128
 DR = 64
 DV = 128
@@ -26,21 +25,6 @@
 BF16 = jnp.bfloat16
 
 
-def rotate(values, positions):
-    half_width = values.shape[-1] // 2
-    frequency = ROPE_THETA ** (-2.0 * jnp.arange(half_width, dtype=jnp.float32) / values.shape[-1])
-    angles = positions.astype(jnp.float32)[:, None] * frequency[None, :]
-    table_shape = (values.shape[0],) + (1,) * (values.ndim - 2) + (half_width,)
-    cosine = jnp.cos(angles).reshape(table_shape)
-    sine_part = jnp.sin(angles).reshape(table_shape)
-    widened = values.astype(jnp.float32)
-    first_half = widened[..., :half_width]
-    second = widened[..., half_width:]
-    return jnp.concatenate(
-        [first_half * cosine - second * sine_part, second * cosine + first_half * sine_part], -1
-    )
-
-
 def layer_norm(values, gain_vec):
     centre = jnp.mean(values, -1, keepdims=True)
     spread = jnp.mean(jnp.square(values - centre), -1, keepdims=True)
@@ -60,6 +44,15 @@
         src_ref=src, dst_ref=dst, send_sem=send_sem, recv_sem=recv_sem,
         device_id=(sp, tp), device_id_type=MESH,
     )
+
+
+def flip(me, d):
+    out, bit = me, 1
+    while bit <= d:
+        if d & bit:
+            out = out + bit * (1 - 2 * (me // bit % 2))
+        bit *= 2
+    return out
 
 
 def greet(devices):
@@ -70,43 +63,66 @@
 
 
 def attention_kernel(
-    n, pack_ref, q_ref, hot_ref, wk_ref, wv_ref, wo_ref, res_ref, gain_ref, out_ref,
-    held, wo_other, scores, vals, att, att_other, send_sem, recv_sem, wo_sem, att_sem,
+    n, lat_ref, tail_ref, qc_ref, qr_ref, cos_ref, sin_ref, wk_ref, wv_ref, wo_ref, res_ref, gain_ref,
+    out_ref, held, held_tail, wo_other, scores, vals, att, att_other, send_sem, recv_sem, tsend_sem, trecv_sem, wo_sem, att_sem,
 ):
     me, tp = lax.axis_index("sp"), lax.axis_index("tp")
-    tok = pack_ref.shape[0]
-    rank = wk_ref.shape[0]
-    heads = q_ref.shape[0]
+    tok = lat_ref.shape[0]
+    heads = qc_ref.shape[1] // DK
     rows = out_ref.shape[0]
-    mine = (me, tp)
-    del mine
     greet(
         [(lax.rem(me + d, n), tp) for d in range(1, REACH + 1)]
         + [(lax.rem(me + n - d, n), tp) for d in range(1, REACH + 1)]
         + [(me, 1 - tp)]
     )
-    copies = [None]
+    copies, tails = [None], [None]
     for d in range(1, REACH + 1):
+        to = lax.rem(me + d, n)
         copies.append(
-            remote(pack_ref, held.at[d - 1], send_sem.at[d - 1], recv_sem.at[d - 1],
-                   lax.rem(me + d, n), tp)
+            remote(lat_ref, held.at[d - 1], send_sem.at[d - 1], recv_sem.at[d - 1], to, tp)
+        )
+        tails.append(
+            remote(tail_ref, held_tail.at[d - 1], tsend_sem.at[d - 1], trecv_sem.at[d - 1], to, tp)
         )
         copies[d].start()
+        tails[d].start()
     share = remote(wo_ref, wo_other, wo_sem.at[0], wo_sem.at[1], me, 1 - tp)
     share.start()
     key_cols = pl.ds(pl.multiple_of(tp * heads * DK, 128), heads * DK)
     value_cols = pl.ds(pl.multiple_of(tp * heads * DV, 128), heads * DV)
     wk = wk_ref[:, key_cols]
     wv = wv_ref[:, value_cols]
-    hot = hot_ref[...]
+    own_tail = tail_ref[...]
+    tail_lane = lax.broadcasted_iota(jnp.int32, own_tail.shape, 1)
+    hot = jnp.where(tail_lane >= DR, own_tail.astype(F32), 0.0).astype(BF16)
+    turned = qr_ref[...]
+    lanes = turned.shape[1]
+    at = lax.broadcasted_iota(jnp.int32, (lanes, lanes), 1)
+    source = lax.broadcasted_iota(jnp.int32, (lanes, lanes), 0)
+    low = lax.rem(at, DR) < DR // 2
+    partner = jnp.where(low, at + DR // 2, at - DR // 2)
+    swap_mat = jnp.where(source == partner, jnp.where(low, -1.0, 1.0), 0.0).astype(BF16)
+    copies_of = lanes // cos_ref.shape[1]
+    cosine = jnp.concatenate([cos_ref[...]] * copies_of, 1)
+    sine = jnp.concatenate([sin_ref[...]] * copies_of, 1)
+    turned = (turned.astype(F32) * cosine + dot(turned, swap_mat) * sine).astype(BF16)
+    wide_at = lax.broadcasted_iota(jnp.int32, (lanes, heads * 128), 1)
+    wide_source = lax.broadcasted_iota(jnp.int32, (lanes, heads * 128), 0)
+    spot = wide_source // DR * 128 + lax.rem(wide_source, DR)
+    spread = jnp.where(wide_at == spot, 1.0, 0.0).astype(BF16)
+    wide_q = dot(turned, spread).astype(BF16)
+    queries = [
+        jnp.concatenate([qc_ref[:, h * DK:(h + 1) * DK], wide_q[:, h * 128:(h + 1) * 128]], 1)
+        for h in range(heads)
+    ]
     for d in range(REACH + 1):
         if d == 0:
-            block = pack_ref[...]
+            lat, tail = lat_ref[...], own_tail
         else:
             copies[d].wait_recv()
-            block = held[d - 1]
+            tails[d].wait_recv()
+            lat, tail = held[d - 1], held_tail[d - 1]
         span = slice((REACH - d) * tok, (REACH - d + 1) * tok)
-        lat, tail = block[:, :rank], block[:, rank:]
         kc = dot(lat, wk).astype(BF16)
         vals[span, :] = dot(lat, wv).astype(BF16)
         allowed = dot_nt(hot, tail) > 0.5
@@ -115,7 +131,7 @@
         allowed = allowed & (k_at <= q_at) & (k_at + me * tok >= 0)
         for h in range(heads):
             key = jnp.concatenate([kc[:, h * DK:(h + 1) * DK], tail], 1)
-            s = dot_nt(q_ref[h], key) * ((DK + DR) ** (-0.5))
+            s = dot_nt(queries[h], key) * ((DK + DR) ** (-0.5))
             scores[h, :, span] = jnp.where(allowed, s, -jnp.inf)
     for h in range(heads):
         s = scores[h]
@@ -134,26 +150,30 @@
     out_ref[...] = layer_norm(total, gain_ref[...]).astype(BF16)
     for d in range(1, REACH + 1):
         copies[d].wait_send()
+        tails[d].wait_send()
     share.wait_send()
     swap.wait_send()
 
 
-def attention(n, pack, q, hot, wk, wv, wo, res, gain):
-    tok, wide = pack.shape
-    heads = q.shape[0]
+def attention(n, latent, tail, qc, qr, cosine, sine, wk, wv, wo, res, gain):
+    tok = latent.shape[0]
+    heads = qc.shape[1] // DK
     rows, width = res.shape
     return pl.pallas_call(
         functools.partial(attention_kernel, n),
         out_shape=jax.ShapeDtypeStruct((rows, width), BF16),
-        in_specs=[VMEM] * 8,
+        in_specs=[VMEM] * 11,
         out_specs=VMEM,
         scratch_shapes=[
-            pltpu.VMEM((REACH, tok, wide), BF16),
+            pltpu.VMEM((REACH,) + latent.shape, BF16),
+            pltpu.VMEM((REACH,) + tail.shape, BF16),
             pltpu.VMEM(wo.shape, BF16),
             pltpu.VMEM((heads, tok, (REACH + 1) * tok), F32),
             pltpu.VMEM(((REACH + 1) * tok, heads * DV), BF16),
             pltpu.VMEM((tok, heads * DV), BF16),
             pltpu.VMEM((rows, heads * DV), BF16),
+            pltpu.SemaphoreType.DMA((REACH,)),
+            pltpu.SemaphoreType.DMA((REACH,)),
             pltpu.SemaphoreType.DMA((REACH,)),
             pltpu.SemaphoreType.DMA((REACH,)),
             pltpu.SemaphoreType.DMA((2,)),
@@ -163,16 +183,16 @@
             collective_id=0, has_side_effects=True, vmem_limit_bytes=40 * 2**20
         ),
         name="attention",
-    )(pack, q, hot, wk, wv, wo, res, gain)
+    )(latent, tail, qc, qr, cosine, sine, wk, wv, wo, res, gain)
 
 
 def expert_kernel(
-    n, cap, normed_ref, placing_ref, pick_ref, weight_ref, gain_ref, wg_hbm, wu_hbm, wd_hbm, out_ref,
+    n, cap, normed_ref, slot_ref, slot_row_ref, weight_ref, gain_ref, wg_hbm, wu_hbm, wd_hbm, out_ref,
     wg, wu, wd, outb, xin, hid, part, recvp, result, returned, total,
     w_sem, send_sem, recv_sem, fsend_sem, frecv_sem, psend_sem, precv_sem, rsend_sem, rrecv_sem,
 ):
     me, tp = lax.axis_index("sp"), lax.axis_index("tp")
-    width = normed_ref.shape[1]
+    rows, width = normed_ref.shape
     hidden = hid.shape[1]
     per = n // CHUNKS
     tall = per * 2 * cap
@@ -184,14 +204,17 @@
         load.start()
     normed = normed_ref[...]
     for c in range(CHUNKS):
-        lines = slice(c * per * cap, (c + 1) * per * cap)
+        line = lax.broadcasted_iota(jnp.int32, (per * cap, rows), 0) + c * per * cap
+        placing = jnp.zeros(line.shape, F32)
+        for k in range(TOPK):
+            placing = jnp.where(line == slot_row_ref[k:k + 1, :], 1.0, placing)
         outb[c * per:(c + 1) * per] = (
-            dot(placing_ref[lines, :], normed).astype(BF16).reshape(per, cap, width)
+            dot(placing.astype(BF16), normed).astype(BF16).reshape(per, cap, width)
         )
     greet([(lax.rem(me + d, n), tp) for d in range(1, n)] + [(me, 1 - tp)])
     sends, forwards, parts, returns = [None], [], [], [None]
     for d in range(1, n):
-        to = lax.rem(me + d, n)
+        to = flip(me, d)
         sends.append(remote(outb.at[to], xin.at[d, tp], send_sem.at[d], recv_sem.at[d], to, tp))
         sends[d].start()
     xin[0, tp] = outb[me]
@@ -206,7 +229,7 @@
                    me, 1 - tp)
         )
     for d in range(1, n):
-        back = lax.rem(me + n - d, n)
+        back = flip(me, d)
         returns.append(
             remote(result.at[d], returned.at[me], rsend_sem.at[d], rrecv_sem.at[d], back, tp)
         )
@@ -261,12 +284,16 @@
     for d in range(1, n):
         returns[d].wait_recv()
     weights = weight_ref[...]
+    slot_at = lax.broadcasted_iota(jnp.int32, (rows, n * cap), 1)
+    picks = [
+        jnp.where(slot_at == slot_ref[:, k:k + 1], 1.0, 0.0).astype(BF16) for k in range(TOPK)
+    ]
     for j in range(width // 512):
         cols = slice(j * 512, (j + 1) * 512)
         rows_back = returned[:, :, cols].reshape(n * cap, 512)
         value = RESIDUAL_SCALE * normed_ref[:, cols].astype(F32)
         for k in range(TOPK):
-            value = value + weights[:, k:k + 1] * dot(pick_ref[k], rows_back)
+            value = value + weights[:, k:k + 1] * dot(picks[k], rows_back)
         total[:, cols] = value
     out_ref[...] = layer_norm(total[...], gain_ref[...]).astype(BF16)
     for d in range(n):
@@ -278,7 +305,7 @@
         parts[c].wait_send()
 
 
-def experts(n, cap, normed, placing, pick, weights, gain, wg, wu, wd):
+def experts(n, cap, normed, slots, slot_rows, weights, gain, wg, wu, wd):
     rows, width = normed.shape
     hidden = wg.shape[1]
     tall = n // CHUNKS * 2 * cap
@@ -314,7 +341,7 @@
             collective_id=1, has_side_effects=True, vmem_limit_bytes=58 * 2**20
         ),
         name="experts",
-    )(normed, placing, pick, weights, gain, wg, wu, wd)
+    )(normed, slots, slot_rows, weights, gain, wg, wu, wd)
 
 
 def per_device(
@@ -336,21 +363,28 @@
     out_gain,
 ):
     tok_dev = latent.shape[0]
-    core_count = lax.axis_size("tp")
     chip_count = lax.axis_size("sp")
-    heads_here = HEADS // core_count
     sp_index = lax.axis_index("sp")
     own_position = sp_index * tok_dev + jnp.arange(tok_dev, dtype=jnp.int32)
-    query_turned = rotate(queries_rotary.reshape(tok_dev, heads_here, DR), own_position).astype(BF16)
-    query_block = queries_content.reshape(tok_dev, heads_here, DK)
-    q = jnp.concatenate([query_block, query_turned, jnp.zeros_like(query_turned)], -1)
-    q = q.transpose(1, 0, 2)
-    key_turned = rotate(rotary_key, own_position).astype(BF16)
+    lane = jnp.arange(128, dtype=jnp.int32) % (DR // 2)
+    frequency = ROPE_THETA ** (-2.0 * lane.astype(F32) / DR)
+    angles = own_position.astype(F32)[:, None] * frequency[None, :]
+    cosine, sine = jnp.cos(angles), jnp.sin(angles)
+    half = DR // 2
+    first, second = rotary_key[:, :half].astype(F32), rotary_key[:, half:].astype(F32)
+    cos_half, sin_half = cosine[:, :half], sine[:, :half]
     hot = (doc_ids[:, None] == jnp.arange(DR, dtype=jnp.int32)[None, :]).astype(BF16)
-    pack = jnp.concatenate([latent, key_turned, hot], 1)
-    hot = jnp.concatenate([jnp.zeros_like(hot), hot], 1)
+    tail = jnp.concatenate(
+        [
+            (first * cos_half - second * sin_half).astype(BF16),
+            (second * cos_half + first * sin_half).astype(BF16),
+            hot,
+        ],
+        1,
+    )
     normed = attention(
-        chip_count, pack, q, hot, w_key_up, w_value_up, w_out, residual, norm_gain[None]
+        chip_count, latent, tail, queries_content, queries_rotary, cosine, sine,
+        w_key_up, w_value_up, w_out, residual, norm_gain[None],
     )
     row_count = normed.shape[0]
     capacity = max(2, 2 * row_count * TOPK // chip_count)
@@ -360,11 +394,8 @@
     )
     slot_rank = jnp.sum((jnp.cumsum(member, 0) - member) * member, 1)
     slot_index = (flat_route * capacity + slot_rank).reshape(row_count, TOPK)
-    slots = jnp.arange(chip_count * capacity, dtype=jnp.int32)
-    pick = (slot_index.T[:, :, None] == slots).astype(BF16)
-    placing = jnp.any(slot_index[None] == slots[:, None, None], -1).astype(BF16)
     return experts(
-        chip_count, capacity, normed, placing, pick, route_weights, out_gain[None],
+        chip_count, capacity, normed, slot_index, slot_index.T, route_weights, out_gain[None],
         w_gate[0], w_up[0], w_down[0],
     )
 

time: 180 us -> 158 us (0.88)
  the two profiles are of different devices: /device:TPU:0 before, /device:TPU:16 now
where the time goes in v2:
time: 158 us; the launch traced here: 156 us
  Pallas kernels  137 us (87%)
  local copies, waits for them, and re-layouts  14.6 us (9%)
  other arithmetic  3.65 us (2%)
    pallas_call x1, Pallas kernels, experts(): pl.pallas_call(functools.partial(expert_kernel, n, cap), out_shape=jax.Sh...  120 us
    pallas_call x1, Pallas kernels, attention(): pl.pallas_call(functools.partial(attention_kernel, n), out_shape=jax.Shap...  17.4 us
    unnamed x24, local copies, waits for them, and re-layouts  13.1 us

profile of v2, /device:TPU:16, one launch (start us, length us, event | category | flops | bytes accessed | tf_op | source)
XLA Modules:
  0.0 155.9 jit_solution(2602765198423564869)
XLA Ops:
  0.0 0.7 slice_convert_fusion
  0.8 0.8 copy.32
  1.5 0.1 eq.47
  1.7 0.1 eq.43
  1.8 0.6 reduce-window.6
  2.4 0.2 slice_reduce_fusion
  2.7 0.1 fusion.7
  2.7 0.1 reduce_sum.12
  2.9 0.1 copy.35
  3.0 0.7 multiply_add_fusion
  3.7 0.0 copy-start.9
  3.7 0.7 copy.36.slot_ref
  4.4 0.1 copy.38
  4.5 0.8 fusion.4
  5.3 1.4 copy.37.weight_ref
  6.7 0.1 copy.29
  6.8 0.5 multiply_cosine_fusion
  7.4 0.1 pad_maximum_fusion.tail_ref
  7.5 0.0 copy-start
  7.5 1.6 %copy-done = bf16[512,2048]{1,0:T(8,128)(2,1)S(1)} copy-done((bf16[512,2048]{1,0:T(8,128)(2,1)S(1)}, bf16[512,2048]{1,0:T(8,128)(2,1)}, u32[]{:S(2)}) %copy-start) | copy-done | bytes 2097176
  9.1 0.0 copy-start.2
  9.1 1.0 copy-done.2
  10.1 0.0 copy-start.3
  10.1 1.0 copy-done.3
  11.2 0.0 copy-start.4
  11.2 1.0 copy-done.4
  12.2 0.0 copy-start.5
  12.2 0.9 copy-done.5
  13.2 0.0 copy-start.6
  13.2 0.9 copy-done.6
  14.1 0.0 copy-start.7
  14.1 0.9 copy-done.7
  15.0 0.0 copy-start.8
  15.0 0.7 copy-done.8
  15.7 17.4 %attention.1.normed_ref = bf16[128,2048]{1,0:T(8,128)(2,1)S(1)} custom-call(bf16[256,256]{1,0:T(8,128)(2,1)S(1)} %copy-done.6, bf16[256,128]{1,0:T(8,128)(2,1)S(1)} %pad_maximum_fusion.tail_ref, bf16[256,512]{1,0:T(8,128)(2,1)S(1)} %copy-done.5, bf16[256,256]{1,0:T(8,128)(2,1)S(1)} %copy-done.7, f32[256,128]{1,0:T(8,128)S(1)} %get-tuple-element.9.cos_ref, ...), custom_call_target="tpu_custom_call" | custom-call | tf_op jit(solution)/shard_map/attention/pallas_call | solution.py:162
  33.1 0.0 copy-done.9
  33.1 0.0 copy-start.1
  33.1 0.8 copy-done.1
  33.9 120.1 %experts.1 = bf16[128,2048]{1,0:T(8,128)(2,1)} custom-call(bf16[128,2048]{1,0:T(8,128)(2,1)} %copy-done.1, s32[128,2]{1,0:T(8,128)} %copy.36.slot_ref, s32[2,128]{1,0:T(2,128)} %bitcast.29, f32[128,2]{1,0:T(8,128)} %copy.37.weight_ref, f32[1,2048]{1,0:T(1,128)} %bitcast.30, bf16[2048,1792]{1,0:T(8,128)(2,1)} %bitcast.26, bf16[2048,1792]{1,0:T(8,128)(2,1)} %bitcast.27, ...), custom_call_target="tpu_custom_call" | custom-call | tf_op jit(solution)/shard_map/experts/pallas_call | solution.py:313
  154.0 1.9 %copy.42 = bf16[128,2048]{1,0:T(8,128)(2,1)} copy(bf16[128,2048]{1,0:T(8,128)(2,1)} %experts.1) | data formatting | bytes 1048576
  (6 shorter events, 0.1 us)
Async XLA Ops:
  3.7 29.4 %copy-start.9 = (s32[128,2]{0,1:T(2,128)}, s32[128,2]{0,1:T(2,128)S(1)}, u32[]{:S(2)}) copy-start(s32[128,2]{0,1:T(2,128)S(1)} %multiply_add_fusion) | copy-start | bytes 3076
  7.5 1.6 %copy-start = (bf16[512,2048]{1,0:T(8,128)(2,1)S(1)}, bf16[512,2048]{1,0:T(8,128)(2,1)}, u32[]{:S(2)}) copy-start(bf16[512,2048]{1,0:T(8,128)(2,1)} %wo_ref.1) | copy-start | bytes 6291460
  9.1 1.0 copy-start.2
  10.1 1.0 copy-start.3
  11.2 1.0 copy-start.4
  12.2 0.9 copy-start.5
  13.2 0.9 copy-start.6
  14.1 0.9 copy-start.7
  15.0 0.7 copy-start.8
  33.1 0.8 copy-start.1
